TPU v7x, 32 devices: a whole 2x2x4 slice. The times are simulated.
32 devices in a mesh: ep: 4 (over y, x), tp: 8 (over z, core).
Axes of the slice: x: 2, y: 2, z: 4, core: 2. Of those that a mesh axis runs over, the one named last changes fastest.
Arguments:
- tokens: bfloat16 [2048, 4096], P('tp', 'ep'), may hold values from -20 to 20
- norm_gain: bfloat16 [4096], P('ep'), may hold values from 0.099609375 to 1.8984375
- expert_ids: int32 [2048, 2], P('tp'), may hold values from 0 to 7, all different within a row; in each aligned block of 256 rows (0 to 255, 256 to 511, ...) at most 128 rows name the same one
- combine_weight: float32 [2048, 2], P('tp'), may hold values from 0.05 to 1
- w_gate: bfloat16 [8, 2048, 4096], P('tp', 'ep'), may hold values from -0.09375 to 0.09375
- w_up: bfloat16 [8, 2048, 4096], P('tp', 'ep'), may hold values from -0.09375 to 0.09375
- w_down: bfloat16 [8, 2048, 4096], P('tp', None, 'ep'), may hold values from -2 to 2
- out_gain: bfloat16 [4096], P('ep'), may hold values from 0.099609375 to 1.8984375
Outputs:
- mixed: bfloat16 [2048, 4096], P('tp', 'ep')
Inputs may be any that keep to these rules, and one draw needn't show every extreme that they name: `expert_ids`: each row names 2 different experts; among the rows of one index of tp no expert is named by more than 128 rows, a bound that some block reaches.
All inputs are finite; a program needn't handle non-finite values.
Results may differ from a plain program's by a relative error of at most 0.007.
Values may be sent and summed in bfloat16 or wider, within the bound.
A program may use at most 64 MiB of HBM per device.

v0:
```python
import functools
import math

import jax
import jax.numpy as jnp
from jax import lax
from jax.experimental import pallas as pl
from jax.experimental.pallas import tpu as pltpu
from jax.sharding import PartitionSpec as P

epsilon = 1e-06
MESH = pl.DeviceIdType.MESH
F32 = jnp.float32
BF16 = jnp.bfloat16


def remote(src, dst, send, recv, dev):
    return pltpu.make_async_remote_copy(
        src_ref=src, dst_ref=dst, send_sem=send, recv_sem=recv, device_id=dev, device_id_type=MESH
    )


def kernel(
    cfg, tok, gain, idst, cwt, og, wg, wu, wd, out,
    wgv, wuv, wdv, X, H, TB, O, R, G, SS, key, KS, KR, acc, wcol,
    wsem, lsend, lrecv, psend, precv, usend, urecv, ksend, krecv, rsend, rrecv, gsend, grecv, ssend, srecv, xsend, xrecv, hsend, hrecv,
):
    n_ep, n_tp, ny, nx, cap, crow = cfg
    nch = n_tp * cap // crow
    grp = max(1, crow // cap)
    cut = max(1, cap // crow)
    piece = cap // cut
    half = crow // 2
    T, wl = tok.shape
    top = idst.shape[0]
    width = wl * n_ep
    fl = wgv.shape[0]
    p = lax.axis_index("ep")
    q = lax.axis_index("tp")
    y, x = p // nx, p % nx

    weights = [
        pltpu.make_async_copy(a, b, wsem.at[k])
        for k, (a, b) in enumerate(((wg.at[0], wgv), (wu.at[0], wuv), (wd.at[0], wdv)))
    ]
    for w in weights:
        w.start()

    nz = n_tp // 2
    z, core = q // 2, q % 2

    def tpp(i):
        res, bit = 0, 1
        while bit < n_tp:
            res = res + ((q // bit + i // bit) % 2) * bit
            bit = bit * 2
        return res

    barrier = pltpu.get_barrier_semaphore()
    for j in range(1, n_ep):
        pl.semaphore_signal(barrier, inc=1, device_id=(lax.rem(p + j, n_ep), q), device_id_type=MESH)
    for i in range(1, n_tp):
        pl.semaphore_signal(barrier, inc=1, device_id=(p, tpp(i)), device_id_type=MESH)

    erow = lax.broadcasted_iota(jnp.int32, (n_tp, T), 0)
    named = jnp.zeros((n_tp, T), F32)
    for k in range(top):
        named = named + jnp.where(idst[k : k + 1, :] == erow, 1.0, 0.0)
    weight = jnp.zeros((128, T), F32)
    wrow = lax.broadcasted_iota(jnp.int32, (128, T), 0)
    for k in range(top):
        weight = weight + jnp.where(idst[k : k + 1, :] == wrow, cwt[k : k + 1, :], 0.0)
    wcol[...] = weight.T
    before = lax.broadcasted_iota(jnp.int32, (T, T), 0) < lax.broadcasted_iota(jnp.int32, (T, T), 1)
    rank = jnp.dot(named.astype(BF16), jnp.where(before, 1.0, 0.0).astype(BF16), preferred_element_type=F32)
    key[...] = jnp.where(named > 0.0, rank, -1.0)
    G[pl.ds(p, 1)] = jnp.broadcast_to(gain[...].astype(F32).reshape(1, wl), (8, wl))[None]

    def onehot(row):
        at = lax.broadcasted_iota(jnp.int32, (cap, T), 0).astype(F32)
        return jnp.where(row == at, 1.0, 0.0).astype(BF16)

    def pick(e):
        return onehot(key[pl.ds(e, 1), :])

    def rows_of(i):
        return pl.ds(pl.multiple_of(i * cap, cap), cap)

    def slot(t):
        late = (t + n_tp - 3) // n_tp
        last = t // (n_tp - 1)
        return t + late - last * (t - 2)

    def keys(i):
        return remote(KS.at[i], KR.at[i], ksend.at[i], krecv.at[i], (p, tpp(i)))

    def right(s):
        return remote(TB.at[s], TB.at[s], lsend.at[s], lrecv.at[s], (p, lax.rem(q + 2, n_tp)))

    def left(s):
        return remote(TB.at[s], TB.at[s], usend.at[s], urecv.at[s], (p, lax.rem(q + n_tp - 2, n_tp)))

    def share(s):
        return remote(TB.at[s], TB.at[s], psend.at[s], precv.at[s], (p, z * 2 + 1 - core))

    def relay(k):
        @pl.when(z - k >= 0)
        def _():
            s = q - 2 * k
            right(s).wait_recv()

            @pl.when(z < nz - 1)
            def _():
                right(s).start()

            share(s).start()

        @pl.when(z + k < nz)
        def _():
            s = q + 2 * k
            left(s).wait_recv()

            @pl.when(z > 0)
            def _():
                left(s).start()

            share(s).start()

    def select(t):
        i = slot(t)
        s = tpp(i)

        @pl.when(i % 2 == 1)
        def _():
            share(s).wait_recv()

        @pl.when(i > 0)
        def _():
            keys(i).wait_recv()

        row = KR[pl.ds(i, 1)][0, 0:1]
        block = jnp.dot(onehot(row), TB[pl.ds(s, 1)][0], preferred_element_type=F32)
        X[y, x, rows_of(t)] = block.astype(BF16)

    def back(i, h):
        part = pl.ds(pl.multiple_of(h * piece, piece), piece)
        return remote(O.at[i, part], R.at[i, part], rsend.at[i, h], rrecv.at[i, h], (p, tpp(i)))

    TB[pl.ds(q, 1)] = tok[...][None]
    KR[0] = jnp.broadcast_to(key[pl.ds(q, 1), :], (8, T))

    def key_rows(i, _):
        KS[pl.ds(i, 1)] = jnp.broadcast_to(key[pl.ds(tpp(i), 1), :], (8, T))[None]
        return 0

    lax.fori_loop(1, n_tp, key_rows, 0)
    pl.semaphore_wait(barrier, n_ep - 1 + n_tp - 1)

    def gcopy(j):
        return remote(G.at[p], G.at[p], gsend.at[j - 1], grecv.at[j - 1], (lax.rem(p + j, n_ep), q))

    def gwait(j):
        o = lax.rem(p - j + n_ep, n_ep)
        return remote(G.at[o], G.at[o], gsend.at[j - 1], grecv.at[j - 1], (lax.rem(p + j, n_ep), q))

    for j in range(1, n_ep):
        gcopy(j).start()

    def send_keys(i, _):
        keys(i).start()
        return 0

    lax.fori_loop(1, n_tp, send_keys, 0)

    @pl.when(z < nz - 1)
    def _():
        right(q).start()

    @pl.when(z > 0)
    def _():
        left(q).start()

    share(q).start()

    def gather(Z, ss, rs):
        def ra(c):
            return pl.ds(pl.multiple_of(c * crow, half), half)

        def rb(c):
            return pl.ds(pl.multiple_of(c * crow + half, half), half)

        def first(c, mine):
            res = []
            for j in range(1, nx):
                o = x if mine else lax.rem(x - j + nx, nx)
                r = Z.at[y, o, ra(c)]
                res.append(remote(r, r, ss.at[0, c, j - 1], rs.at[0, c, j - 1], (y * nx + lax.rem(x + j, nx), q)))
            for j in range(1, ny):
                o = y if mine else lax.rem(y - j + ny, ny)
                r = Z.at[o, x, rb(c)]
                res.append(remote(r, r, ss.at[1, c, j - 1], rs.at[1, c, j - 1], (lax.rem(y + j, ny) * nx + x, q)))
            return res

        def second(c, mine):
            res = []
            for j in range(1, ny):
                o = y if mine else lax.rem(y - j + ny, ny)
                r = Z.at[o, :, ra(c)]
                res.append(remote(r, r, ss.at[2, c, j - 1], rs.at[2, c, j - 1], (lax.rem(y + j, ny) * nx + x, q)))
            for j in range(1, nx):
                o = x if mine else lax.rem(x - j + nx, nx)
                r = Z.at[:, o, rb(c)]
                res.append(remote(r, r, ss.at[3, c, j - 1], rs.at[3, c, j - 1], (y * nx + lax.rem(x + j, nx), q)))
            return res

        return first, second

    x1, x2 = gather(X, xsend, xrecv)
    h1, h2 = gather(H, hsend, hrecv)

    def start(copies):
        for c in copies:
            c.start()

    def recv(copies):
        for c in copies:
            c.wait_recv()

    for t in range(1, grp):
        if slot(t) % 2 == 0:
            relay(slot(t) // 2)
    acc[...] = jnp.zeros_like(acc)

    def crows(c):
        return pl.ds(pl.multiple_of(c * crow, crow), crow)

    def hidden(c):
        total = jnp.zeros((crow, 1), F32)
        for a in range(ny):
            for b in range(nx):
                v = X[a, b, crows(c)].astype(F32)
                total = total + jnp.sum(v * v, axis=1, keepdims=True)
        scale = lax.rsqrt(total / width + epsilon)
        gate = jnp.zeros((crow, fl), F32)
        up = jnp.zeros((crow, fl), F32)
        for a in range(ny):
            for b in range(nx):
                o = a * nx + b
                v = (X[a, b, crows(c)].astype(F32) * scale * G[o, 0:1]).astype(BF16)
                dims = (((1,), (1,)), ((), ()))
                gate = gate + lax.dot_general(v, wgv[:, o * wl : (o + 1) * wl], dims, preferred_element_type=F32)
                up = up + lax.dot_general(v, wuv[:, o * wl : (o + 1) * wl], dims, preferred_element_type=F32)
        H[y, x, crows(c)] = (gate / (1.0 + jnp.exp(-gate)) * up).astype(BF16)

    def down(c):
        res = jnp.zeros((crow, wl), F32)
        for a in range(ny):
            for b in range(nx):
                o = a * nx + b
                res = res + jnp.dot(H[a, b, crows(c)], wdv[o * fl : (o + 1) * fl, :], preferred_element_type=F32)
        return res.astype(BF16)

    def combine(i):
        e = tpp(i)
        lane = lax.broadcasted_iota(jnp.int32, (T, 128), 1)
        weight = jnp.sum(jnp.where(lane == e, wcol[...], 0.0), axis=1, keepdims=True)
        part = lax.dot_general(pick(e), R[i], (((0,), (0,)), ((), ())), preferred_element_type=F32)
        acc[...] += weight * part

    def step(t, _):
        @pl.when(t < nch)
        def _():
            @pl.when(t % cut == 0)
            def _():
                for g in range(grp):
                    select(t // cut * grp + g)

            start(x1(t, True))

        @pl.when((t >= 1) & (t < nch + 1))
        def _():
            recv(x1(t - 1, False))
            start(x2(t - 1, True))

        @pl.when((t >= 3) & (t < nch + 3))
        def _():
            recv(h1(t - 3, False))
            start(h2(t - 3, True))

        @pl.when((t >= 2) & (t < nch + 2))
        def _():
            @pl.when(t == 2)
            def _():
                weights[0].wait()
                weights[1].wait()
                for j in range(1, n_ep):
                    gwait(j).wait_recv()

            recv(x2(t - 2, False))
            hidden(t - 2)
            start(h1(t - 2, True))

        @pl.when((t >= 4) & (t < nch + 4))
        def _():
            @pl.when(t == 4)
            def _():
                weights[2].wait()

            recv(h2(t - 4, False))
            res = down(t - 4)
            for g in range(grp):
                i = slot((t - 4) // cut * grp + g)
                h = (t - 4) % cut
                part = pl.ds(pl.multiple_of(h * piece, piece), piece)
                O[pl.ds(i, 1), part] = res[g * piece : (g + 1) * piece][None]

                @pl.when(i > 0)
                def _():
                    back(i, h).start()

                @pl.when(i == 0)
                def _():
                    R[0, part] = res[g * piece : (g + 1) * piece]

        @pl.when((t + 1 < nch) & ((t + 1) % cut == 0))
        def _():
            for g in range(grp):
                i = slot((t + 1) // cut * grp + g)

                @pl.when(i % 2 == 0)
                def _():
                    relay(i // 2)

        @pl.when((t >= 6) & ((t - 6) % cut == cut - 1))
        def _():
            for g in range(grp):
                i = slot((t - 6) // cut * grp + g)

                @pl.when(i > 0)
                def _():
                    for h in range(cut):
                        back(i, h).wait_recv()

                combine(i)

        return 0

    lax.fori_loop(0, nch + 6, step, 0)

    moe = acc[...]
    mine = jnp.sum(moe * moe, axis=1, keepdims=True)
    SS[pl.ds(p, 1)] = jnp.broadcast_to(mine, (T, 128)).T[0:8][None]

    def scopy(j, o):
        return remote(SS.at[o], SS.at[o], ssend.at[j - 1], srecv.at[j - 1], (lax.rem(p + j, n_ep), q))

    for j in range(1, n_ep):
        scopy(j, p).start()

    def drain_tp(i, _):
        keys(i).wait_send()
        for h in range(cut):
            back(i, h).wait_send()
        return 0

    lax.fori_loop(1, n_tp, drain_tp, 0)

    def drain_z(zs, _):
        s = zs * 2 + core
        share(s).wait_send()

        @pl.when((zs <= z) & (z < nz - 1))
        def _():
            right(s).wait_send()

        @pl.when((zs >= z) & (z > 0))
        def _():
            left(s).wait_send()

        return 0

    lax.fori_loop(0, nz, drain_z, 0)

    def drain_ep(c, _):
        for w in x1(c, True) + x2(c, True) + h1(c, True) + h2(c, True):
            w.wait_send()
        return 0

    lax.fori_loop(0, nch, drain_ep, 0)
    for j in range(1, n_ep):
        gcopy(j).wait_send()
    for j in range(1, n_ep):
        scopy(j, p).wait_send()
        scopy(j, lax.rem(p - j + n_ep, n_ep)).wait_recv()
    total = SS[0]
    for o in range(1, n_ep):
        total = total + SS[o]
    column = jnp.broadcast_to(total[0:1], (128, T)).T[:, 0:1]
    out[...] = (moe * lax.rsqrt(column / width + epsilon) * og[...].astype(F32).reshape(1, wl)).astype(BF16)


def body(tokens, norm_gain, expert_ids, combine_weight, w_gate, w_up, w_down, out_gain):
    T, wl = tokens.shape
    n_ep = lax.axis_size("ep")
    n_tp = lax.axis_size("tp")
    top = expert_ids.shape[1]
    cap = 2 * top * T // n_tp
    fl = w_gate.shape[1]
    width = wl * n_ep
    root = math.isqrt(n_ep)
    ny, nx = (root, root) if root * root == n_ep else (1, n_ep)
    rows = n_tp * cap
    crow = 64
    cut = max(1, cap // crow)
    nch = rows // crow
    peers = max(1, nx - 1, ny - 1)
    cfg = (n_ep, n_tp, ny, nx, cap, crow)
    vm = pl.BlockSpec(memory_space=pltpu.VMEM)
    anym = pl.BlockSpec(memory_space=pl.ANY)
    dma = pltpu.SemaphoreType.DMA
    return pl.pallas_call(
        functools.partial(kernel, cfg),
        out_shape=jax.ShapeDtypeStruct((T, wl), BF16),
        in_specs=[vm] * 5 + [anym] * 3,
        out_specs=vm,
        scratch_shapes=[
            pltpu.VMEM((fl, width), BF16),
            pltpu.VMEM((fl, width), BF16),
            pltpu.VMEM((fl * n_ep, wl), BF16),
            pltpu.VMEM((ny, nx, rows, wl), BF16),
            pltpu.VMEM((ny, nx, rows, fl), BF16),
            pltpu.VMEM((n_tp, T, wl), BF16),
            pltpu.VMEM((n_tp, cap, wl), BF16),
            pltpu.VMEM((n_tp, cap, wl), BF16),
            pltpu.VMEM((n_ep, 8, wl), F32),
            pltpu.VMEM((n_ep, 8, T), F32),
            pltpu.VMEM((n_tp, T), F32),
            pltpu.VMEM((n_tp, 8, T), F32),
            pltpu.VMEM((n_tp, 8, T), F32),
            pltpu.VMEM((T, wl), F32),
            pltpu.VMEM((T, 128), F32),
            dma((3,)),
            dma((n_tp,)), dma((n_tp,)), dma((n_tp,)), dma((n_tp,)),
            dma((n_tp,)), dma((n_tp,)), dma((n_tp,)), dma((n_tp,)),
            dma((n_tp, cut)), dma((n_tp, cut)),
            dma((n_ep,)), dma((n_ep,)), dma((n_ep,)), dma((n_ep,)),
            dma((4, nch, peers)), dma((4, nch, peers)), dma((4, nch, peers)), dma((4, nch, peers)),
        ],
        compiler_params=pltpu.CompilerParams(
            collective_id=0, has_side_effects=True, vmem_limit_bytes=60 * 1024 * 1024
        ),
        name="moe",
    )(
        tokens, norm_gain, expert_ids.T, combine_weight.T, out_gain,
        w_gate, w_up, w_down,
    )


def solution(mesh):
    return jax.shard_map(
        body,
        mesh=mesh,
        in_specs=(
            P("tp", "ep"),
            P("ep"),
            P("tp", None),
            P("tp", None),
            P("tp", "ep", None),
            P("tp", "ep", None),
            P("tp", None, "ep"),
            P("ep"),
        ),
        out_specs=P("tp", "ep"),
        check_vma=False,
    )
```

profile of v0, /device:TPU:0, one launch (start us, length us, event | category | flops | bytes accessed | tf_op | source)
XLA Modules:
  0.0 132.5 jit_solution(9931991202462194827)
XLA Ops:
  0.0 130.6 %moe.1 = bf16[256,1024]{1,0:T(8,128)(2,1)} custom-call(bf16[256,1024]{1,0:T(8,128)(2,1)} %tok.1, bf16[1024]{0:T(1024)(128)(2,1)} %gain.1, s32[2,256]{1,0:T(2,128)} %bitcast.2, f32[2,256]{1,0:T(2,128)} %bitcast.3, bf16[1024]{0:T(1024)(128)(2,1)} %og.1, bf16[1,512,4096]{2,1,0:T(8,128)(2,1)} %wg.1, bf16[1,512,4096]{2,1,0:T(8,128)(2,1)} %wu.1, ...), custom_call_target="tpu_custom_call" | custom-call | tf_op jit(solution)/shard_map/moe/pallas_call | solution.py:421
  130.6 1.9 %copy.10 = bf16[256,1024]{1,0:T(8,128)(2,1)} copy(bf16[256,1024]{1,0:T(8,128)(2,1)} %moe.1) | data formatting | bytes 1048576
where the time goes:
time: 134 us; the launch traced here: 132 us
  Pallas kernels  131 us (98%)
  local copies, waits for them, and re-layouts  1.87 us (1%)
    pallas_call x1, Pallas kernels, body(): pl.pallas_call(functools.partial(kernel, cfg), out_shape=jax.ShapeDtypeSt...  131 us

commit v1 on v0

v1 whole, which is shorter than its diff:
```python
import functools
import math

import jax
import jax.numpy as jnp
from jax import lax
from jax.experimental import pallas as pl
from jax.experimental.pallas import tpu as pltpu
from jax.sharding import PartitionSpec as P

epsilon = 1e-06
MESH = pl.DeviceIdType.MESH
F32 = jnp.float32
BF16 = jnp.bfloat16


def remote(src, dst, send, recv, dev):
    return pltpu.make_async_remote_copy(
        src_ref=src, dst_ref=dst, send_sem=send, recv_sem=recv, device_id=dev, device_id_type=MESH
    )


def kernel(
    cfg, tok, gain, idst, cwt, og, wg, wu, wd, out,
    wgv, wuv, wdv, X, H, TB, O, R, G, SS, V, key, KS, KR, acc, wcol,
    wsem, lsend, lrecv, psend, precv, usend, urecv, ksend, krecv, rsend, rrecv, gsend, grecv, ssend, srecv, xsend, xrecv, hsend, hrecv,
):
    n_ep, n_tp, ny, nx, cap, crow, cols = cfg
    nch = n_tp * cap // crow
    grp = max(1, crow // cap)
    cut = max(1, cap // crow)
    piece = cap // cut
    half = crow // 2
    units = nch // cut
    T, wl = tok.shape
    pw = wl // cols
    top = idst.shape[0]
    width = wl * n_ep
    fl = wgv.shape[0]
    p = lax.axis_index("ep")
    q = lax.axis_index("tp")
    y, x = p // nx, p % nx

    weights = [
        pltpu.make_async_copy(a, b, wsem.at[k])
        for k, (a, b) in enumerate(((wg.at[0], wgv), (wu.at[0], wuv), (wd.at[0], wdv)))
    ]
    for w in weights:
        w.start()

    nz = n_tp // 2
    z, core = q // 2, q % 2

    def tpp(i):
        res, bit = 0, 1
        while bit < n_tp:
            res = res + ((q // bit + i // bit) % 2) * bit
            bit = bit * 2
        return res

    barrier = pltpu.get_barrier_semaphore()
    for j in range(1, n_ep):
        pl.semaphore_signal(barrier, inc=1, device_id=(lax.rem(p + j, n_ep), q), device_id_type=MESH)
    for i in range(1, n_tp):
        pl.semaphore_signal(barrier, inc=1, device_id=(p, tpp(i)), device_id_type=MESH)

    erow = lax.broadcasted_iota(jnp.int32, (n_tp, T), 0)
    named = jnp.zeros((n_tp, T), F32)
    for k in range(top):
        named = named + jnp.where(idst[k : k + 1, :] == erow, 1.0, 0.0)
    weight = jnp.zeros((128, T), F32)
    wrow = lax.broadcasted_iota(jnp.int32, (128, T), 0)
    for k in range(top):
        weight = weight + jnp.where(idst[k : k + 1, :] == wrow, cwt[k : k + 1, :], 0.0)
    wcol[...] = weight.T
    before = lax.broadcasted_iota(jnp.int32, (T, T), 0) < lax.broadcasted_iota(jnp.int32, (T, T), 1)
    rank = jnp.dot(named.astype(BF16), jnp.where(before, 1.0, 0.0).astype(BF16), preferred_element_type=F32)
    key[...] = jnp.where(named > 0.0, rank, -1.0)
    G[pl.ds(p, 1)] = jnp.broadcast_to(gain[...].astype(F32).reshape(1, wl), (8, wl))[None]

    def onehot(row):
        at = lax.broadcasted_iota(jnp.int32, (cap, T), 0).astype(F32)
        return jnp.where(row == at, 1.0, 0.0).astype(BF16)

    def pick(e):
        return onehot(key[pl.ds(e, 1), :])

    def rows_of(i):
        return pl.ds(pl.multiple_of(i * cap, cap), cap)

    def seek(table, k):
        res = k + table[0]
        for i in range(1, units):
            jump = table[i] - table[i - 1] - 1
            if jump:
                res = res + (k + units - i) // units * jump
        return res

    def line(head, tail):
        return head + [u for u in range(units) if u not in head + tail] + tail

    xorder = line([0, 1, 2], [3])
    horder = line([0, 2], [1, 3])
    reach = [0]
    for u in xorder:
        reach.append(max(reach[-1], (u * grp + grp - 1) // 2))

    def xchunk(t):
        return seek(xorder, t // cut) * cut + t % cut

    def hchunk(t):
        return seek(horder, t // cut) * cut + t % cut

    def part(j):
        return pl.ds(j * pw, pw)

    def keys(i):
        return remote(KS.at[i], KR.at[i], ksend.at[i], krecv.at[i], (p, tpp(i)))

    def right(s, j):
        b = TB.at[s, :, part(j)]
        return remote(b, b, lsend.at[s, j], lrecv.at[s, j], (p, lax.rem(q + 2, n_tp)))

    def left(s, j):
        b = TB.at[s, :, part(j)]
        return remote(b, b, usend.at[s, j], urecv.at[s, j], (p, lax.rem(q + n_tp - 2, n_tp)))

    def share(s, j):
        b = TB.at[s, :, part(j)]
        return remote(b, b, psend.at[s, j], precv.at[s, j], (p, z * 2 + 1 - core))

    def relay(k, j):
        @pl.when(z - k >= 0)
        def _():
            s = q - 2 * k
            right(s, j).wait_recv()

            @pl.when(z < nz - 1)
            def _():
                right(s, j).start()

            share(s, j).start()

        @pl.when(z + k < nz)
        def _():
            s = q + 2 * k
            left(s, j).wait_recv()

            @pl.when(z > 0)
            def _():
                left(s, j).start()

            share(s, j).start()

    def select(i, j):
        s = tpp(i)

        @pl.when(i % 2 == 1)
        def _():
            share(s, j).wait_recv()

        if j == 0:

            @pl.when(i > 0)
            def _():
                keys(i).wait_recv()

        row = KR[pl.ds(i, 1)][0, 0:1]
        block = jnp.dot(onehot(row), TB[pl.ds(s, 1), :, part(j)][0], preferred_element_type=F32)
        X[y, x, rows_of(i), part(j)] = block.astype(BF16)

    def fetch(k, j):
        lo = seek(reach[:-1], k) + 1
        hi = seek(reach[1:], k) + 1
        lax.fori_loop(lo, hi, lambda r, a: (relay(r, j), a)[1], 0)
        for g in range(grp):
            select(seek(xorder, k) * grp + g, j)

    def back(i, h):
        rows = pl.ds(pl.multiple_of(h * piece, piece), piece)
        return remote(O.at[i, rows], R.at[i, rows], rsend.at[i, h], rrecv.at[i, h], (p, tpp(i)))

    TB[pl.ds(q, 1)] = tok[...][None]
    KR[0] = jnp.broadcast_to(key[pl.ds(q, 1), :], (8, T))

    def key_rows(i, _):
        KS[pl.ds(i, 1)] = jnp.broadcast_to(key[pl.ds(tpp(i), 1), :], (8, T))[None]
        return 0

    lax.fori_loop(1, n_tp, key_rows, 0)
    for j in range(cols):
        select(0, j)
    pl.semaphore_wait(barrier, n_ep - 1 + n_tp - 1)

    def gcopy(j):
        return remote(G.at[p], G.at[p], gsend.at[j - 1], grecv.at[j - 1], (lax.rem(p + j, n_ep), q))

    def gwait(j):
        o = lax.rem(p - j + n_ep, n_ep)
        return remote(G.at[o], G.at[o], gsend.at[j - 1], grecv.at[j - 1], (lax.rem(p + j, n_ep), q))

    def gather(Z, ss, rs, wide):
        def ra(c):
            return pl.ds(pl.multiple_of(c * crow, half), half)

        def rb(c):
            return pl.ds(pl.multiple_of(c * crow + half, half), half)

        def send(k, c, n, j, r, dev):
            return remote(r, r, ss.at[k, c, n - 1, j], rs.at[k, c, n - 1, j], dev)

        def across(n):
            return (y * nx + lax.rem(x + n, nx), q)

        def along(n):
            return (lax.rem(y + n, ny) * nx + x, q)

        def first(c, mine, j=0):
            res = []
            w = pl.ds(j * wide, wide)
            for n in range(1, nx):
                o = x if mine else lax.rem(x - n + nx, nx)
                res.append(send(0, c, n, j, Z.at[y, o, ra(c), w], across(n)))
            for n in range(1, ny):
                o = y if mine else lax.rem(y - n + ny, ny)
                res.append(send(1, c, n, j, Z.at[o, x, rb(c), w], along(n)))
            return res

        def second(c, mine, j=0):
            res = []
            w = pl.ds(j * wide, wide)
            for n in range(1, ny):
                o = y if mine else lax.rem(y - n + ny, ny)
                res.append(send(2, c, n, j, Z.at[o, :, ra(c), w], along(n)))
            for n in range(1, nx):
                o = x if mine else lax.rem(x - n + nx, nx)
                res.append(send(3, c, n, j, Z.at[:, o, rb(c), w], across(n)))
            return res

        return first, second

    x1, x2 = gather(X, xsend, xrecv, wl)
    h1, h2 = gather(H, hsend, hrecv, fl)

    def start(copies):
        for c in copies:
            c.start()

    def recv(copies):
        for c in copies:
            c.wait_recv()

    def send_keys(i, _):
        keys(i).start()
        return 0

    lax.fori_loop(1, n_tp, send_keys, 0)
    for j in range(cols):

        @pl.when(z < nz - 1)
        def _():
            right(q, j).start()

        @pl.when(z > 0)
        def _():
            left(q, j).start()

        share(q, j).start()
        for g in range(1, grp):
            select(g, j)
        if j == 0 and grp == 1:
            start(x1(0, True))
    if grp > 1:
        start(x1(0, True))
    for j in range(1, n_ep):
        gcopy(j).start()
    acc[...] = jnp.zeros_like(acc)

    def crows(c):
        return pl.ds(pl.multiple_of(c * crow, crow), crow)

    def hidden(c):
        total = jnp.zeros((crow, 1), F32)
        for a in range(ny):
            for b in range(nx):
                v = X[a, b, crows(c)].astype(F32)
                total = total + jnp.sum(v * v, axis=1, keepdims=True)
        scale = lax.rsqrt(total / width + epsilon)
        for a in range(ny):
            for b in range(nx):
                o = a * nx + b
                v = X[a, b, crows(c)].astype(F32) * scale * G[o, 0:1]
                V[:, o * wl : (o + 1) * wl] = v.astype(BF16)
        dims = (((1,), (1,)), ((), ()))
        gate = lax.dot_general(V[...], wgv[...], dims, preferred_element_type=F32)
        up = lax.dot_general(V[...], wuv[...], dims, preferred_element_type=F32)
        H[y, x, crows(c)] = (gate / (1.0 + jnp.exp(-gate)) * up).astype(BF16)

    def down(c):
        res = jnp.zeros((crow, wl), F32)
        for a in range(ny):
            for b in range(nx):
                o = a * nx + b
                res = res + jnp.dot(H[a, b, crows(c)], wdv[o * fl : (o + 1) * fl, :], preferred_element_type=F32)
        return res.astype(BF16)

    def combine(i):
        e = tpp(i)
        lane = lax.broadcasted_iota(jnp.int32, (T, 128), 1)
        weight = jnp.sum(jnp.where(lane == e, wcol[...], 0.0), axis=1, keepdims=True)
        term = lax.dot_general(pick(e), R[i], (((0,), (0,)), ((), ())), preferred_element_type=F32)
        acc[...] += weight * term

    def step(t, _):
        @pl.when((t >= 8) & (t < nch + 8))
        def _():
            @pl.when(t == 8)
            def _():
                weights[2].wait()

            c = hchunk(t - 8)
            recv(h2(c, False))
            res = down(c)
            for g in range(grp):
                i = seek(horder, (t - 8) // cut) * grp + g
                h = (t - 8) % cut
                rows = pl.ds(pl.multiple_of(h * piece, piece), piece)
                O[pl.ds(i, 1), rows] = res[g * piece : (g + 1) * piece][None]

                @pl.when(i > 0)
                def _():
                    back(i, h).start()

                @pl.when(i == 0)
                def _():
                    R[0, rows] = res[g * piece : (g + 1) * piece]

        @pl.when((t >= 5) & (t < nch + 5))
        def _():
            @pl.when(t == 5)
            def _():
                weights[0].wait()
                weights[1].wait()
                for j in range(1, n_ep):
                    gwait(j).wait_recv()

            c = hchunk(t - 5)
            recv(x2(c, False))
            hidden(c)
            start(h1(c, True))

        @pl.when((t >= 6) & (t < nch + 6))
        def _():
            c = hchunk(t - 6)
            recv(h1(c, False))
            start(h2(c, True))

        @pl.when(t < nch)
        def _():
            @pl.when(t % cut == 0)
            def _():
                for j in range(cols):
                    fetch(t // cut, j)

            start(x1(xchunk(t), True))

        @pl.when((t >= 15) & (t < nch + 15) & ((t - 15) % cut == cut - 1))
        def _():
            for g in range(grp):
                i = seek(horder, (t - 15) // cut) * grp + g

                @pl.when(i > 0)
                def _():
                    for h in range(cut):
                        back(i, h).wait_recv()

                combine(i)

        @pl.when((t >= 1) & (t < nch + 1))
        def _():
            c = xchunk(t - 1)
            recv(x1(c, False))
            start(x2(c, True))

        return 0

    lax.fori_loop(1, nch + 15, step, 0)

    moe = acc[...]
    mine = jnp.sum(moe * moe, axis=1, keepdims=True)
    SS[pl.ds(p, 1)] = jnp.broadcast_to(mine, (T, 128)).T[0:8][None]

    def scopy(j, o):
        return remote(SS.at[o], SS.at[o], ssend.at[j - 1], srecv.at[j - 1], (lax.rem(p + j, n_ep), q))

    for j in range(1, n_ep):
        scopy(j, p).start()

    def drain_tp(i, _):
        keys(i).wait_send()
        for h in range(cut):
            back(i, h).wait_send()
        return 0

    lax.fori_loop(1, n_tp, drain_tp, 0)

    def drain_z(zs, _):
        s = zs * 2 + core
        for j in range(cols):
            share(s, j).wait_send()

            @pl.when((zs <= z) & (z < nz - 1))
            def _():
                right(s, j).wait_send()

            @pl.when((zs >= z) & (z > 0))
            def _():
                left(s, j).wait_send()

        return 0

    lax.fori_loop(0, nz, drain_z, 0)

    def drain_ep(c, _):
        for w in x1(c, True) + x2(c, True) + h1(c, True) + h2(c, True):
            w.wait_send()
        return 0

    lax.fori_loop(0, nch, drain_ep, 0)
    for j in range(1, n_ep):
        gcopy(j).wait_send()
    for j in range(1, n_ep):
        scopy(j, p).wait_send()
        scopy(j, lax.rem(p - j + n_ep, n_ep)).wait_recv()
    total = SS[0]
    for o in range(1, n_ep):
        total = total + SS[o]
    column = jnp.broadcast_to(total[0:1], (128, T)).T[:, 0:1]
    out[...] = (moe * lax.rsqrt(column / width + epsilon) * og[...].astype(F32).reshape(1, wl)).astype(BF16)


def body(tokens, norm_gain, expert_ids, combine_weight, w_gate, w_up, w_down, out_gain):
    T, wl = tokens.shape
    n_ep = lax.axis_size("ep")
    n_tp = lax.axis_size("tp")
    top = expert_ids.shape[1]
    cap = 2 * top * T // n_tp
    fl = w_gate.shape[1]
    width = wl * n_ep
    root = math.isqrt(n_ep)
    ny, nx = (root, root) if root * root == n_ep else (1, n_ep)
    rows = n_tp * cap
    crow = 64
    cut = max(1, cap // crow)
    nch = rows // crow
    peers = max(1, nx - 1, ny - 1)
    cols = 2 if wl % 256 == 0 else 1
    cfg = (n_ep, n_tp, ny, nx, cap, crow, cols)
    vm = pl.BlockSpec(memory_space=pltpu.VMEM)
    anym = pl.BlockSpec(memory_space=pl.ANY)
    dma = pltpu.SemaphoreType.DMA
    return pl.pallas_call(
        functools.partial(kernel, cfg),
        out_shape=jax.ShapeDtypeStruct((T, wl), BF16),
        in_specs=[vm] * 5 + [anym] * 3,
        out_specs=vm,
        scratch_shapes=[
            pltpu.VMEM((fl, width), BF16),
            pltpu.VMEM((fl, width), BF16),
            pltpu.VMEM((fl * n_ep, wl), BF16),
            pltpu.VMEM((ny, nx, rows, wl), BF16),
            pltpu.VMEM((ny, nx, rows, fl), BF16),
            pltpu.VMEM((n_tp, T, wl), BF16),
            pltpu.VMEM((n_tp, cap, wl), BF16),
            pltpu.VMEM((n_tp, cap, wl), BF16),
            pltpu.VMEM((n_ep, 8, wl), F32),
            pltpu.VMEM((n_ep, 8, T), F32),
            pltpu.VMEM((crow, width), BF16),
            pltpu.VMEM((n_tp, T), F32),
            pltpu.VMEM((n_tp, 8, T), F32),
            pltpu.VMEM((n_tp, 8, T), F32),
            pltpu.VMEM((T, wl), F32),
            pltpu.VMEM((T, 128), F32),
            dma((3,)),
            dma((n_tp, cols)), dma((n_tp, cols)), dma((n_tp, cols)), dma((n_tp, cols)),
            dma((n_tp, cols)), dma((n_tp, cols)), dma((n_tp,)), dma((n_tp,)),
            dma((n_tp, cut)), dma((n_tp, cut)),
            dma((n_ep,)), dma((n_ep,)), dma((n_ep,)), dma((n_ep,)),
            dma((4, nch, peers, 1)), dma((4, nch, peers, 1)), dma((4, nch, peers, 1)), dma((4, nch, peers, 1)),
        ],
        compiler_params=pltpu.CompilerParams(
            collective_id=0, has_side_effects=True, vmem_limit_bytes=60 * 1024 * 1024
        ),
        name="moe",
    )(
        tokens, norm_gain, expert_ids.T, combine_weight.T, out_gain,
        w_gate, w_up, w_down,
    )


def solution(mesh):
    return jax.shard_map(
        body,
        mesh=mesh,
        in_specs=(
            P("tp", "ep"),
            P("ep"),
            P("tp", None),
            P("tp", None),
            P("tp", "ep", None),
            P("tp", "ep", None),
            P("tp", None, "ep"),
            P("ep"),
        ),
        out_specs=P("tp", "ep"),
        check_vma=False,
    )
```

time: 134 us -> 131 us (0.978); the launches traced: 132 us -> 131 us
  Pallas kernels: 131 us -> 129 us
    pallas_call x1, Pallas kernels: 131 us -> 129 us  [body(): pl.pallas_call(functools.partial(kernel, cfg), out_shape=jax.ShapeDtypeSt...]
where the time goes in v1:
time: 131 us
  Pallas kernels  129 us (98%)
  local copies, waits for them, and re-layouts  1.87 us (1%)
    pallas_call x1, Pallas kernels, body(): pl.pallas_call(functools.partial(kernel, cfg), out_shape=jax.ShapeDtypeSt...  129 us

profile of v1, /device:TPU:0, one launch (start us, length us, event | category | flops | bytes accessed | tf_op | source)
XLA Modules:
  0.0 130.8 jit_solution(1097155736185180267)
XLA Ops:
  0.0 129.0 %moe.1 = bf16[256,1024]{1,0:T(8,128)(2,1)} custom-call(bf16[256,1024]{1,0:T(8,128)(2,1)} %tok.1, bf16[1024]{0:T(1024)(128)(2,1)} %gain.1, s32[2,256]{1,0:T(2,128)} %bitcast.2, f32[2,256]{1,0:T(2,128)} %bitcast.3, bf16[1024]{0:T(1024)(128)(2,1)} %og.1, bf16[1,512,4096]{2,1,0:T(8,128)(2,1)} %wg.1, bf16[1,512,4096]{2,1,0:T(8,128)(2,1)} %wu.1, ...), custom_call_target="tpu_custom_call" | custom-call | tf_op jit(solution)/shard_map/moe/pallas_call | solution.py:462
  129.0 1.9 %copy.10 = bf16[256,1024]{1,0:T(8,128)(2,1)} copy(bf16[256,1024]{1,0:T(8,128)(2,1)} %moe.1) | data formatting | bytes 1048576

commit v2 on v1

--- a/solution.py
+++ b/solution.py
@@ -22,7 +22,7 @@
 
 def kernel(
     cfg, tok, gain, idst, cwt, og, wg, wu, wd, out,
-    wgv, wuv, wdv, X, H, TB, O, R, G, SS, V, key, KS, KR, acc, wcol,
+    wgv, wuv, wdv, X, H, TB, O, R, G, SS, V, WT, key, KS, KR, acc, wcol,
     wsem, lsend, lrecv, psend, precv, usend, urecv, ksend, krecv, rsend, rrecv, gsend, grecv, ssend, srecv, xsend, xrecv, hsend, hrecv,
 ):
     n_ep, n_tp, ny, nx, cap, crow, cols = cfg
@@ -100,7 +100,7 @@
         return head + [u for u in range(units) if u not in head + tail] + tail
 
     xorder = line([0, 1, 2], [3])
-    horder = line([0, 2], [1, 3])
+    horder = line([0, 2], [1, units - 1, 3])
     reach = [0]
     for u in xorder:
         reach.append(max(reach[-1], (u * grp + grp - 1) // 2))
@@ -291,9 +291,8 @@
                 o = a * nx + b
                 v = X[a, b, crows(c)].astype(F32) * scale * G[o, 0:1]
                 V[:, o * wl : (o + 1) * wl] = v.astype(BF16)
-        dims = (((1,), (1,)), ((), ()))
-        gate = lax.dot_general(V[...], wgv[...], dims, preferred_element_type=F32)
-        up = lax.dot_general(V[...], wuv[...], dims, preferred_element_type=F32)
+        gate = jnp.dot(V[...], WT[0], preferred_element_type=F32)
+        up = jnp.dot(V[...], WT[1], preferred_element_type=F32)
         H[y, x, crows(c)] = (gate / (1.0 + jnp.exp(-gate)) * up).astype(BF16)
 
     def down(c):
@@ -312,6 +311,27 @@
         acc[...] += weight * term
 
     def step(t, _):
+        @pl.when((t >= 5) & (t < nch + 5))
+        def _():
+            @pl.when(t == 5)
+            def _():
+                for j in range(1, n_ep):
+                    gwait(j).wait_recv()
+
+            c = hchunk(t - 5)
+            recv(x2(c, False))
+            hidden(c)
+            start(h1(c, True))
+
+        @pl.when(t < nch)
+        def _():
+            @pl.when(t % cut == 0)
+            def _():
+                for j in range(cols):
+                    fetch(t // cut, j)
+
+            start(x1(xchunk(t), True))
+
         @pl.when((t >= 8) & (t < nch + 8))
         def _():
             @pl.when(t == 8)
@@ -335,39 +355,10 @@
                 def _():
                     R[0, rows] = res[g * piece : (g + 1) * piece]
 
-        @pl.when((t >= 5) & (t < nch + 5))
-        def _():
-            @pl.when(t == 5)
-            def _():
-                weights[0].wait()
-                weights[1].wait()
-                for j in range(1, n_ep):
-                    gwait(j).wait_recv()
-
-            c = hchunk(t - 5)
-            recv(x2(c, False))
-            hidden(c)
-            start(h1(c, True))
-
-        @pl.when((t >= 6) & (t < nch + 6))
-        def _():
-            c = hchunk(t - 6)
-            recv(h1(c, False))
-            start(h2(c, True))
-
-        @pl.when(t < nch)
-        def _():
-            @pl.when(t % cut == 0)
-            def _():
-                for j in range(cols):
-                    fetch(t // cut, j)
-
-            start(x1(xchunk(t), True))
-
-        @pl.when((t >= 15) & (t < nch + 15) & ((t - 15) % cut == cut - 1))
+        @pl.when((t >= 17) & (t < nch + 17) & ((t - 17) % cut == cut - 1))
         def _():
             for g in range(grp):
-                i = seek(horder, (t - 15) // cut) * grp + g
+                i = seek(horder, (t - 17) // cut) * grp + g
 
                 @pl.when(i > 0)
                 def _():
@@ -376,15 +367,36 @@
 
                 combine(i)
 
+        @pl.when((t >= 6) & (t < nch + 6))
+        def _():
+            c = hchunk(t - 6)
+            recv(h1(c, False))
+            start(h2(c, True))
+
         @pl.when((t >= 1) & (t < nch + 1))
         def _():
             c = xchunk(t - 1)
             recv(x1(c, False))
             start(x2(c, True))
 
+        @pl.when(t < 5)
+        def _():
+            @pl.when(t == 1)
+            def _():
+                weights[0].wait()
+                weights[1].wait()
+
+            def turn(b, _):
+                at = pl.ds(pl.multiple_of((t - 1) * (width // 4) + b * 256, 256), 256)
+                WT[0, at] = wgv[:, at].T
+                WT[1, at] = wuv[:, at].T
+                return 0
+
+            lax.fori_loop(0, width // 1024, turn, 0)
+
         return 0
 
-    lax.fori_loop(1, nch + 15, step, 0)
+    lax.fori_loop(1, nch + 17, step, 0)
 
     moe = acc[...]
     mine = jnp.sum(moe * moe, axis=1, keepdims=True)
@@ -476,6 +488,7 @@
             pltpu.VMEM((n_ep, 8, wl), F32),
             pltpu.VMEM((n_ep, 8, T), F32),
             pltpu.VMEM((crow, width), BF16),
+            pltpu.VMEM((2, width, fl), BF16),
             pltpu.VMEM((n_tp, T), F32),
             pltpu.VMEM((n_tp, 8, T), F32),
             pltpu.VMEM((n_tp, 8, T), F32),

time: 131 us -> 129 us (0.985)
  Pallas kernels: 129 us -> 127 us
    pallas_call x1, Pallas kernels: 129 us -> 127 us  [body(): pl.pallas_call(functools.partial(kernel, cfg), out_shape=jax.ShapeDtypeSt...]
where the time goes in v2:
time: 129 us
  Pallas kernels  127 us (98%)
  local copies, waits for them, and re-layouts  1.87 us (1%)
    pallas_call x1, Pallas kernels, body(): pl.pallas_call(functools.partial(kernel, cfg), out_shape=jax.ShapeDtypeSt...  127 us

profile of v2, /device:TPU:0, one launch (start us, length us, event | category | flops | bytes accessed | tf_op | source)
XLA Modules:
  0.0 128.9 jit_solution(9900676046157015261)
XLA Ops:
  0.0 127.1 %moe.1 = bf16[256,1024]{1,0:T(8,128)(2,1)} custom-call(bf16[256,1024]{1,0:T(8,128)(2,1)} %tok.1, bf16[1024]{0:T(1024)(128)(2,1)} %gain.1, s32[2,256]{1,0:T(2,128)} %bitcast.2, f32[2,256]{1,0:T(2,128)} %bitcast.3, bf16[1024]{0:T(1024)(128)(2,1)} %og.1, bf16[1,512,4096]{2,1,0:T(8,128)(2,1)} %wg.1, bf16[1,512,4096]{2,1,0:T(8,128)(2,1)} %wu.1, ...), custom_call_target="tpu_custom_call" | custom-call | tf_op jit(solution)/shard_map/moe/pallas_call | solution.py:474
  127.1 1.9 %copy.10 = bf16[256,1024]{1,0:T(8,128)(2,1)} copy(bf16[256,1024]{1,0:T(8,128)(2,1)} %moe.1) | data formatting | bytes 1048576

commit v3 on v2

--- a/solution.py
+++ b/solution.py
@@ -22,18 +22,19 @@
 
 def kernel(
     cfg, tok, gain, idst, cwt, og, wg, wu, wd, out,
-    wgv, wuv, wdv, X, H, TB, O, R, G, SS, V, WT, key, KS, KR, acc, wcol,
-    wsem, lsend, lrecv, psend, precv, usend, urecv, ksend, krecv, rsend, rrecv, gsend, grecv, ssend, srecv, xsend, xrecv, hsend, hrecv,
+    wgv, wuv, wdv, X, H, TB, O, R, G, SS, V, WT, DB, key, KS, KR, acc, wcol,
+    wsem, lsend, lrecv, psend, precv, usend, urecv, ksend, krecv, rsend, rrecv, gsend, grecv, ssend, srecv, xsend, xrecv, hsend, hrecv, dsend, drecv, msend, mrecv,
 ):
-    n_ep, n_tp, ny, nx, cap, crow, cols = cfg
+    n_ep, n_tp, ny, nx, cap, crow, cols, wb = cfg
     nch = n_tp * cap // crow
     grp = max(1, crow // cap)
     cut = max(1, cap // crow)
     piece = cap // cut
-    half = crow // 2
     units = nch // cut
     T, wl = tok.shape
     pw = wl // cols
+    wa = wl - wb
+    early = 4 if wb else 0
     top = idst.shape[0]
     width = wl * n_ep
     fl = wgv.shape[0]
@@ -99,8 +100,8 @@
     def line(head, tail):
         return head + [u for u in range(units) if u not in head + tail] + tail
 
-    xorder = line([0, 1, 2], [3])
-    horder = line([0, 2], [1, units - 1, 3])
+    xorder = line([], [3])
+    horder = line([0, 1], [units - 2, 2, units - 1, 3])
     reach = [0]
     for u in xorder:
         reach.append(max(reach[-1], (u * grp + grp - 1) // 2))
@@ -181,6 +182,8 @@
         return remote(O.at[i, rows], R.at[i, rows], rsend.at[i, h], rrecv.at[i, h], (p, tpp(i)))
 
     TB[pl.ds(q, 1)] = tok[...][None]
+    if wb:
+        DB[0, y, x] = tok[:, wa:]
     KR[0] = jnp.broadcast_to(key[pl.ds(q, 1), :], (8, T))
 
     def key_rows(i, _):
@@ -199,12 +202,14 @@
         o = lax.rem(p - j + n_ep, n_ep)
         return remote(G.at[o], G.at[o], gsend.at[j - 1], grecv.at[j - 1], (lax.rem(p + j, n_ep), q))
 
-    def gather(Z, ss, rs, wide):
+    def gather(Z, ss, rs, wide, rows):
+        half = rows // 2
+
         def ra(c):
-            return pl.ds(pl.multiple_of(c * crow, half), half)
+            return pl.ds(pl.multiple_of(c * rows, half), half)
 
         def rb(c):
-            return pl.ds(pl.multiple_of(c * crow + half, half), half)
+            return pl.ds(pl.multiple_of(c * rows + half, half), half)
 
         def send(k, c, n, j, r, dev):
             return remote(r, r, ss.at[k, c, n - 1, j], rs.at[k, c, n - 1, j], dev)
@@ -239,12 +244,46 @@
 
         return first, second
 
-    x1, x2 = gather(X, xsend, xrecv, wl)
-    h1, h2 = gather(H, hsend, hrecv, fl)
+    thin = gather(X, xsend, xrecv, wa, crow)
+    wide = gather(X, xsend, xrecv, wl, crow)
+    h1, h2 = gather(H, hsend, hrecv, fl, crow)
+    if wb:
+        d1, d2 = gather(DB.at[0], dsend, drecv, wb, T)
+
+    def move(act, k, c, mine):
+        if wb == 0:
+            act(wide[k](c, mine))
+            return
+
+        @pl.when(c // cut < early)
+        def _():
+            act(thin[k](c, mine))
+
+        @pl.when(c // cut >= early)
+        def _():
+            act(wide[k](c, mine))
+
+    def pass_on(src, dst, i):
+        res = []
+        for n in range(1, n_ep):
+            o = lax.rem(p + n, n_ep)
+            res.append(remote(DB.at[src, o // nx, o % nx], DB.at[dst, o // nx, o % nx], msend.at[dst, o], mrecv.at[dst, o], (p, tpp(i))))
+        return res
+
+    def blend(i):
+        row = KR[pl.ds(i, 1)][0, 0:1]
+        for n in range(1, n_ep):
+            o = lax.rem(p + n, n_ep)
+            block = jnp.dot(onehot(row), DB[pl.ds(i, 1), o // nx, o % nx][0], preferred_element_type=F32)
+            X[o // nx, o % nx, rows_of(i), pl.ds(wa, wb)] = block.astype(BF16)
 
     def start(copies):
         for c in copies:
             c.start()
+
+    def sent(copies):
+        for c in copies:
+            c.wait_send()
 
     def recv(copies):
         for c in copies:
@@ -269,9 +308,11 @@
         for g in range(1, grp):
             select(g, j)
         if j == 0 and grp == 1:
-            start(x1(0, True))
+            move(start, 0, 0, True)
+            if wb:
+                start(d1(0, True))
     if grp > 1:
-        start(x1(0, True))
+        move(start, 0, 0, True)
     for j in range(1, n_ep):
         gcopy(j).start()
     acc[...] = jnp.zeros_like(acc)
@@ -311,15 +352,52 @@
         acc[...] += weight * term
 
     def step(t, _):
-        @pl.when((t >= 5) & (t < nch + 5))
-        def _():
+        if wb:
+
+            @pl.when(t == 3)
+            def _():
+                recv(d1(0, False))
+                start(d2(0, True))
+
             @pl.when(t == 5)
+            def _():
+                recv(d2(0, False))
+                start(pass_on(0, 1, 1))
+
+            @pl.when(t == 9)
+            def _():
+                start(pass_on(0, 2, 2))
+
+        @pl.when((t >= 6) & (t < nch + 6))
+        def _():
+            @pl.when(t == 6)
             def _():
                 for j in range(1, n_ep):
                     gwait(j).wait_recv()
 
-            c = hchunk(t - 5)
-            recv(x2(c, False))
+            c = hchunk(t - 6)
+            move(recv, 1, c, False)
+            if wb:
+
+                @pl.when((c // cut < early) & (c % cut == 0))
+                def _():
+                    u = c // cut
+
+                    @pl.when(u == 1)
+                    def _():
+                        recv(pass_on(0, 1, 1))
+
+                    @pl.when(u == 2)
+                    def _():
+                        recv(pass_on(0, 2, 2))
+                        start(pass_on(2, 3, 1))
+
+                    @pl.when(u == 3)
+                    def _():
+                        recv(pass_on(2, 3, 1))
+
+                    blend(u)
+
             hidden(c)
             start(h1(c, True))
 
@@ -330,20 +408,20 @@
                 for j in range(cols):
                     fetch(t // cut, j)
 
-            start(x1(xchunk(t), True))
-
-        @pl.when((t >= 8) & (t < nch + 8))
-        def _():
-            @pl.when(t == 8)
+            move(start, 0, xchunk(t), True)
+
+        @pl.when((t >= 9) & (t < nch + 9))
+        def _():
+            @pl.when(t == 9)
             def _():
                 weights[2].wait()
 
-            c = hchunk(t - 8)
+            c = hchunk(t - 9)
             recv(h2(c, False))
             res = down(c)
             for g in range(grp):
-                i = seek(horder, (t - 8) // cut) * grp + g
-                h = (t - 8) % cut
+                i = seek(horder, (t - 9) // cut) * grp + g
+                h = (t - 9) % cut
                 rows = pl.ds(pl.multiple_of(h * piece, piece), piece)
                 O[pl.ds(i, 1), rows] = res[g * piece : (g + 1) * piece][None]
 
@@ -367,17 +445,17 @@
 
                 combine(i)
 
-        @pl.when((t >= 6) & (t < nch + 6))
-        def _():
-            c = hchunk(t - 6)
+        @pl.when((t >= 7) & (t < nch + 7))
+        def _():
+            c = hchunk(t - 7)
             recv(h1(c, False))
             start(h2(c, True))
 
         @pl.when((t >= 1) & (t < nch + 1))
         def _():
             c = xchunk(t - 1)
-            recv(x1(c, False))
-            start(x2(c, True))
+            move(recv, 0, c, False)
+            move(start, 1, c, True)
 
         @pl.when(t < 5)
         def _():
@@ -434,11 +512,14 @@
     lax.fori_loop(0, nz, drain_z, 0)
 
     def drain_ep(c, _):
-        for w in x1(c, True) + x2(c, True) + h1(c, True) + h2(c, True):
-            w.wait_send()
+        move(sent, 0, c, True)
+        move(sent, 1, c, True)
+        sent(h1(c, True) + h2(c, True))
         return 0
 
     lax.fori_loop(0, nch, drain_ep, 0)
+    if wb:
+        sent(d1(0, True) + d2(0, True) + pass_on(0, 1, 1) + pass_on(0, 2, 2) + pass_on(2, 3, 1))
     for j in range(1, n_ep):
         gcopy(j).wait_send()
     for j in range(1, n_ep):
@@ -467,7 +548,8 @@
     nch = rows // crow
     peers = max(1, nx - 1, ny - 1)
     cols = 2 if wl % 256 == 0 else 1
-    cfg = (n_ep, n_tp, ny, nx, cap, crow, cols)
+    wb = wl * 5 // 8 // 128 * 128 if cap >= crow else 0
+    cfg = (n_ep, n_tp, ny, nx, cap, crow, cols, wb)
     vm = pl.BlockSpec(memory_space=pltpu.VMEM)
     anym = pl.BlockSpec(memory_space=pl.ANY)
     dma = pltpu.SemaphoreType.DMA
@@ -489,6 +571,7 @@
             pltpu.VMEM((n_ep, 8, T), F32),
             pltpu.VMEM((crow, width), BF16),
             pltpu.VMEM((2, width, fl), BF16),
+            pltpu.VMEM((4, ny, nx, T, wb) if wb else (8, 128), BF16),
             pltpu.VMEM((n_tp, T), F32),
             pltpu.VMEM((n_tp, 8, T), F32),
             pltpu.VMEM((n_tp, 8, T), F32),
@@ -500,6 +583,7 @@
             dma((n_tp, cut)), dma((n_tp, cut)),
             dma((n_ep,)), dma((n_ep,)), dma((n_ep,)), dma((n_ep,)),
             dma((4, nch, peers, 1)), dma((4, nch, peers, 1)), dma((4, nch, peers, 1)), dma((4, nch, peers, 1)),
+            dma((4, 1, peers, 1)), dma((4, 1, peers, 1)), dma((4, n_ep)), dma((4, n_ep)),
         ],
         compiler_params=pltpu.CompilerParams(
             collective_id=0, has_side_effects=True, vmem_limit_bytes=60 * 1024 * 1024

time: 129 us -> 127 us (0.984)
  Pallas kernels: 127 us -> 125 us
    pallas_call x1, Pallas kernels: 127 us -> 125 us  [body(): pl.pallas_call(functools.partial(kernel, cfg), out_shape=jax.ShapeDtypeSt...]
where the time goes in v3:
time: 127 us
  Pallas kernels  125 us (98%)
  local copies, waits for them, and re-layouts  1.87 us (1%)
    pallas_call x1, Pallas kernels, body(): pl.pallas_call(functools.partial(kernel, cfg), out_shape=jax.ShapeDtypeSt...  125 us

profile of v3, /device:TPU:0, one launch (start us, length us, event | category | flops | bytes accessed | tf_op | source)
XLA Modules:
  0.0 126.7 jit_solution(17491725921958394775)
XLA Ops:
  0.0 124.8 %moe.1 = bf16[256,1024]{1,0:T(8,128)(2,1)} custom-call(bf16[256,1024]{1,0:T(8,128)(2,1)} %tok.1, bf16[1024]{0:T(1024)(128)(2,1)} %gain.1, s32[2,256]{1,0:T(2,128)} %bitcast.2, f32[2,256]{1,0:T(2,128)} %bitcast.3, bf16[1024]{0:T(1024)(128)(2,1)} %og.1, bf16[1,512,4096]{2,1,0:T(8,128)(2,1)} %wg.1, bf16[1,512,4096]{2,1,0:T(8,128)(2,1)} %wu.1, ...), custom_call_target="tpu_custom_call" | custom-call | tf_op jit(solution)/shard_map/moe/pallas_call | solution.py:556
  124.8 1.9 %copy.10 = bf16[256,1024]{1,0:T(8,128)(2,1)} copy(bf16[256,1024]{1,0:T(8,128)(2,1)} %moe.1) | data formatting | bytes 1048576

commit v4 on v3

--- a/solution.py
+++ b/solution.py
@@ -548,7 +548,7 @@
     nch = rows // crow
     peers = max(1, nx - 1, ny - 1)
     cols = 2 if wl % 256 == 0 else 1
-    wb = wl * 5 // 8 // 128 * 128 if cap >= crow else 0
+    wb = wl * 6 // 8 // 128 * 128 if cap >= crow else 0
     cfg = (n_ep, n_tp, ny, nx, cap, crow, cols, wb)
     vm = pl.BlockSpec(memory_space=pltpu.VMEM)
     anym = pl.BlockSpec(memory_space=pl.ANY)

time: 127 us -> 126 us (level)
  no operation moved by 1% of the time
where the time goes in v4:
time: 126 us; the launch traced here: 125 us
  Pallas kernels  124 us (98%)
  local copies, waits for them, and re-layouts  1.87 us (1%)
    pallas_call x1, Pallas kernels, body(): pl.pallas_call(functools.partial(kernel, cfg), out_shape=jax.ShapeDtypeSt...  124 us

profile of v4, /device:TPU:0, one launch (start us, length us, event | category | flops | bytes accessed | tf_op | source)
XLA Modules:
  0.0 125.5 jit_solution(15558641409577061174)
XLA Ops:
  0.0 123.6 %moe.1 = bf16[256,1024]{1,0:T(8,128)(2,1)} custom-call(bf16[256,1024]{1,0:T(8,128)(2,1)} %tok.1, bf16[1024]{0:T(1024)(128)(2,1)} %gain.1, s32[2,256]{1,0:T(2,128)} %bitcast.2, f32[2,256]{1,0:T(2,128)} %bitcast.3, bf16[1024]{0:T(1024)(128)(2,1)} %og.1, bf16[1,512,4096]{2,1,0:T(8,128)(2,1)} %wg.1, bf16[1,512,4096]{2,1,0:T(8,128)(2,1)} %wu.1, ...), custom_call_target="tpu_custom_call" | custom-call | tf_op jit(solution)/shard_map/moe/pallas_call | solution.py:556
  123.6 1.9 %copy.10 = bf16[256,1024]{1,0:T(8,128)(2,1)} copy(bf16[256,1024]{1,0:T(8,128)(2,1)} %moe.1) | data formatting | bytes 1048576
